TPU v7x, 256 devices: a whole 4x4x8 slice. The times are simulated.
256 devices in a mesh: sp: 64 (over z, x, core), tp: 4 (over y).
Axes of the slice: x: 4, y: 4, z: 8, core: 2. Of those that a mesh axis runs over, the one named last changes fastest.
Arguments:
- stream: bfloat16 [32768, 2048], P(('sp', 'tp')), may hold values from -6 to 6
- broad_queries: bfloat16 [32768, 512], P('sp', 'tp'), may hold values from -6 to 6
- broad_keys: bfloat16 [32768, 512], P('sp', 'tp'), may hold values from -6 to 6
- broad_values: bfloat16 [32768, 1024], P('sp', 'tp'), may hold values from -6 to 6
- broad_output_gate: bfloat16 [32768, 1024], P('sp', 'tp'), may hold values from -6 to 6
- broad_input_gate: float32 [4, 32768], P('tp', 'sp'), may hold values from -6 to 130
- broad_forget_logits: float32 [4, 32768], P('tp', 'sp'), may hold values from 0 to 20
- broad_forget_boost: float32 [4, 32768], P('tp', 'sp'), may hold values from -1 to 0
- slim_queries: bfloat16 [32768, 512], P('sp', 'tp'), may hold values from -6 to 6
- slim_keys: bfloat16 [32768, 512], P('sp', 'tp'), may hold values from -6 to 6
- slim_values: bfloat16 [32768, 1024], P('sp', 'tp'), may hold values from -6 to 6
- slim_output_gate: bfloat16 [32768, 1024], P('sp', 'tp'), may hold values from -6 to 6
- slim_input_gate: float32 [8, 32768], P('tp', 'sp'), may hold values from -6 to 130
- slim_forget_logits: float32 [8, 32768], P('tp', 'sp'), may hold values from 0 to 20
- slim_forget_boost: float32 [8, 32768], P('tp', 'sp'), may hold values from -1 to 0
- broad_output_weight: bfloat16 [1024, 2048], P('tp'), may hold values from -0.125 to 0.125
- slim_output_weight: bfloat16 [1024, 2048], P('tp'), may hold values from -0.125 to 0.125
- expert_norm_gain: float32 [2048], replicated, may hold values from 0.1 to 1.9
- routes: int32 [32768, 2], P('sp'), may hold values from 0 to 63, all different within a row; in each aligned block of 128 rows (0 to 127, 128 to 255, ...) at most 8 rows name the same one
- routing_weight: float32 [32768, 2], P(('sp', 'tp')), may hold values from 0.2 to 1
- expert_gate_weight: bfloat16 [64, 2048, 2048], P('sp', None, 'tp'), may hold values from -0.375 to 0.375
- expert_linear_weight: bfloat16 [64, 2048, 2048], P('sp', None, 'tp'), may hold values from -0.375 to 0.375
- expert_down_weight: bfloat16 [64, 2048, 2048], P('sp', 'tp'), may hold values from -0.01953125 to 0.01953125
Outputs:
- block_out: bfloat16 [32768, 2048], P(('sp', 'tp'))
Inputs may be any that keep to these rules, and one draw needn't show every extreme that they name: `routes`: in each aligned block of 128 rows, a row names 2 different experts and no expert is named by more than 8 rows; every expert is named somewhere.
All inputs are finite; a program needn't handle non-finite values.
Results may differ from a plain program's by a relative error of at most 0.015.
Values may be sent and summed in bfloat16 or wider, within the bound.
No kernel may reach another device: no remote copies, remote signals or barrier semaphores. Data moves between devices by JAX's collectives and lax.ppermute only.
A program may use at most 128 MiB of HBM per device.

v0:
```python
import math

import jax
import jax.numpy as jnp
from jax import lax
from jax.sharding import Mesh
from jax.sharding import PartitionSpec as P

SP = ("sp_0", "sp_1", "sp_2")
SP_TP = ("sp_0", "sp_1", "sp_2", "tp")


EPSILON = 1e-06
FLOOR_LOG = -1e30
LIMIT = 7.0
SLOPE = 1.702
TOP_PRECISION = lax.Precision.HIGHEST


def nothing_yet(x, identity):
    return jax.tree.map(
        lambda a, e: jnp.broadcast_to(jnp.asarray(e, a.dtype), a.shape), x, identity
    )


def collected_together(x, axis):
    leaves = jax.tree.leaves(x)
    order = sorted(range(len(leaves)), key=lambda k: -leaves[k].size)
    width = (1, *leaves[order[0]].shape)[-1]
    lines = [
        jnp.pad(leaves[k].reshape(-1), (0, -leaves[k].size % width)).reshape(-1, width)
        for k in order
    ]
    both, at, found = (lax.all_gather(jnp.concatenate(lines), axis), 0, {})
    for k, line in zip(order, lines):
        slab = both[:, at : at + len(line)].reshape(len(both), -1)
        found[k] = slab[:, : leaves[k].size].reshape(-1, *leaves[k].shape)
        at += len(line)
    numbers = iter(range(len(leaves)))
    return jax.tree.map(lambda _: found[next(numbers)], x)


def prefix_by_axis(x, axes, combine, identity):
    before = start = nothing_yet(x, identity)
    subtotal = x
    for axis in reversed(axes):
        count, place = (lax.axis_size(axis), lax.axis_index(axis))
        pieces = collected_together(subtotal, axis)
        inside, subtotal = (start, start)
        for k in range(count):
            passed = k < place
            subtotal = combine(subtotal, jax.tree.map(lambda part: part[k], pieces))
            inside = jax.tree.map(lambda new, old: jnp.where(passed, new, old), subtotal, inside)
        before = combine(inside, before)
    return before


def in_blocks(x, dim, count):
    before, after = (x.shape[:dim], x.shape[dim + 1 :])
    return jnp.moveaxis(x.reshape(*before, count, -1, *after), dim, 0)


def sent_and_summed(x, axis, dim):
    parts = in_blocks(x, dim, lax.axis_size(axis))
    arrived = lax.all_to_all(parts, axis, split_axis=0, concat_axis=0, tiled=True)
    return arrived.astype(jnp.float32).sum(axis=0)


def summarize(key_rows, value_rows, input_gate_log, log_forget):
    key_size = key_rows.shape[2]
    prefix = jnp.cumsum(log_forget, axis=1)
    totals = prefix[:, -1]
    spread = totals[:, None] - prefix + input_gate_log
    local_max = jnp.max(spread, axis=1)
    weights = jnp.exp(spread - local_max[:, None])
    scaled = key_rows.astype(jnp.float32) / math.sqrt(key_size)
    weighted_output = (jnp.transpose(weights)[:, :, None] * scaled).astype(jnp.bfloat16)
    matrix_memory = jnp.einsum(
        "zqi,zqs->qis", weighted_output, value_rows, preferred_element_type=jnp.float32
    )
    return (totals, local_max, matrix_memory)


def merge_states(earlier, later):
    first_total, first_max, first_memory = earlier
    second_total, second_max, second_memory = later
    new_max = jnp.maximum(second_total + first_max, second_max)
    old_scale = jnp.exp(second_total + first_max - new_max)
    new_scale = jnp.exp(second_max - new_max)
    return (
        first_total + second_total,
        new_max,
        old_scale[:, None, None] * first_memory + new_scale[:, None, None] * second_memory,
    )


def merge_pair(earlier, later):
    return merge_states(earlier[:3], later[:3]) + merge_states(earlier[3:], later[3:])


def read_out(query_rows, key_rows, value_rows, input_gate_log, log_forget, state):
    matrix_memory, carried_max = state
    key_size = key_rows.shape[2]
    length = query_rows.shape[0]
    prefix = jnp.cumsum(log_forget, axis=1)
    causal = lax.broadcasted_iota(jnp.int32, (length, length), 0) >= lax.broadcasted_iota(
        jnp.int32, (length, length), 1
    )
    decays = jnp.where(
        causal[None], prefix[:, :, None] - prefix[:, None, :] + input_gate_log[:, None, :], -jnp.inf
    )
    carried_log = prefix + carried_max[:, None]
    row_max = jnp.maximum(carried_log, jnp.max(decays, axis=2))
    scores = jnp.einsum(
        "thk,shk->hts", query_rows, key_rows, preferred_element_type=jnp.float32
    ) / math.sqrt(key_size)
    weights = jnp.exp(decays - row_max[:, :, None]) * scores
    carried_route_weight = jnp.exp(carried_log - row_max)
    widened_query = query_rows.astype(jnp.float32)
    memory_numerator = carried_route_weight[:, :, None] * jnp.einsum(
        "ldm,dmb->dlb", widened_query, matrix_memory, precision=TOP_PRECISION
    )
    return memory_numerator + jnp.einsum(
        "hts,shv->htv", weights.astype(jnp.bfloat16), value_rows, preferred_element_type=jnp.float32
    )


def gate_out(cells, output_gate_logits):
    head_total, length, width = cells.shape
    square = jnp.mean(cells * cells, axis=2, keepdims=True)
    normed = cells * lax.rsqrt(square + EPSILON)
    normed = jnp.transpose(normed, (1, 0, 2)).reshape(length, head_total * width)
    return (normed * jax.nn.sigmoid(output_gate_logits.astype(jnp.float32))).astype(jnp.bfloat16)


def prepare_inputs(query_rows, key_rows, value_rows, forget_logits, forget_boost):
    head_total = forget_logits.shape[0]
    length = query_rows.shape[0]
    return (
        query_rows.reshape(length, head_total, -1),
        key_rows.reshape(length, head_total, -1),
        value_rows.reshape(length, head_total, -1),
        jax.nn.log_sigmoid(forget_logits) + forget_boost,
    )


def start_state(parts):
    head_total = parts[3].shape[0]
    key_size = parts[1].shape[2]
    value_size = parts[2].shape[2]
    return (
        jnp.zeros((head_total,), jnp.float32),
        jnp.full((head_total,), FLOOR_LOG, jnp.float32),
        jnp.zeros((head_total, key_size, value_size), jnp.float32),
    )


def slot_table(block_routes, experts, capacity):
    rows, top = block_routes.shape
    entries = rows * top
    flat = block_routes.reshape(entries)
    onehot = (flat[:, None] == jnp.arange(experts, dtype=jnp.int32)[None, :]).astype(jnp.float32)
    lower = (
        lax.broadcasted_iota(jnp.int32, (entries, entries), 0)
        > lax.broadcasted_iota(jnp.int32, (entries, entries), 1)
    ).astype(jnp.float32)
    before = jnp.dot(lower, onehot, precision=TOP_PRECISION)
    ranks = jnp.sum(before * onehot, axis=1).astype(jnp.int32)
    slots = flat * capacity + ranks
    matches = slots[None, :] == jnp.arange(experts * capacity, dtype=jnp.int32)[:, None]
    owners = jnp.arange(entries, dtype=jnp.int32) // top
    source = jnp.sum(jnp.where(matches, owners[None, :] + 1, 0), axis=1) - 1
    return (slots, source)


def on_device(
    stream,
    broad_queries,
    broad_keys,
    broad_values,
    broad_output_gate,
    broad_input_gate,
    broad_forget_logits,
    broad_forget_boost,
    slim_queries,
    slim_keys,
    slim_values,
    slim_output_gate,
    slim_input_gate,
    slim_forget_logits,
    slim_forget_boost,
    broad_output_weight,
    slim_output_weight,
    expert_norm_gain,
    routes,
    routing_weight,
    expert_gate_weight,
    expert_linear_weight,
    expert_down_weight,
):
    broad_group = prepare_inputs(
        broad_queries, broad_keys, broad_values, broad_forget_logits, broad_forget_boost
    )
    slim_group = prepare_inputs(
        slim_queries, slim_keys, slim_values, slim_forget_logits, slim_forget_boost
    )
    broad_total, broad_max, broad_memory = summarize(
        broad_group[1], broad_group[2], broad_input_gate, broad_group[3]
    )
    slim_total, slim_max, slim_memory = summarize(
        slim_group[1], slim_group[2], slim_input_gate, slim_group[3]
    )
    identity = start_state(broad_group) + start_state(slim_group)
    incoming = prefix_by_axis(
        (broad_total, broad_max, broad_memory, slim_total, slim_max, slim_memory),
        SP,
        merge_pair,
        identity,
    )
    cells_broad = read_out(
        broad_group[0],
        broad_group[1],
        broad_group[2],
        broad_input_gate,
        broad_group[3],
        (incoming[2], incoming[1]),
    )
    cells_slim = read_out(
        slim_group[0],
        slim_group[1],
        slim_group[2],
        slim_input_gate,
        slim_group[3],
        (incoming[5], incoming[4]),
    )
    broad_mixed_output = gate_out(cells_broad, broad_output_gate)
    slim_mixed_output = gate_out(cells_slim, slim_output_gate)
    tp_count = lax.axis_size("tp")
    tok_dev = broad_queries.shape[0]
    rows = tok_dev // tp_count
    head_sum = sent_and_summed(
        (
            jnp.dot(broad_mixed_output, broad_output_weight, preferred_element_type=jnp.float32)
            + jnp.dot(slim_mixed_output, slim_output_weight, preferred_element_type=jnp.float32)
        ).astype(jnp.bfloat16),
        "tp",
        0,
    )
    middle = (stream.astype(jnp.float32) + head_sum).astype(jnp.bfloat16)
    middle_wide = middle.astype(jnp.float32)
    normed = (
        middle_wide
        * lax.rsqrt(jnp.mean(middle_wide * middle_wide, axis=1, keepdims=True) + EPSILON)
        * expert_norm_gain
    ).astype(jnp.bfloat16)
    width = normed.shape[1]
    experts = lax.axis_size(SP)
    top = routes.shape[1]
    capacity = max(2, 2 * tok_dev * top // (tp_count * experts))
    own_index = lax.axis_index("tp")
    own_routes = lax.dynamic_slice_in_dim(routes, own_index * rows, rows, 0)
    own_slots, own_source = slot_table(own_routes, experts, capacity)
    padded = jnp.concatenate([normed, jnp.zeros((1, width), jnp.bfloat16)], axis=0)
    picks = jnp.where(own_source < 0, rows, own_source)
    outgoing = padded[picks].reshape(experts, capacity, width)
    arrived = lax.all_to_all(outgoing, SP, split_axis=0, concat_axis=0, tiled=True)
    piece = lax.all_gather(arrived[None], "tp", axis=0, tiled=True)
    flat_rows = piece.reshape(-1, width)
    gate_pre = jnp.dot(flat_rows, expert_gate_weight[0], preferred_element_type=jnp.float32)
    lin_pre = jnp.dot(flat_rows, expert_linear_weight[0], preferred_element_type=jnp.float32)
    glu = jnp.minimum(gate_pre, LIMIT)
    linear = jnp.clip(lin_pre, -LIMIT, LIMIT)
    active = (glu * jax.nn.sigmoid(SLOPE * glu) * (linear + 1.0)).astype(jnp.bfloat16)
    partial_out = jnp.dot(
        active, expert_down_weight[0], preferred_element_type=jnp.float32
    ).reshape(piece.shape)
    summed = lax.psum_scatter(
        partial_out.astype(jnp.bfloat16), "tp", scatter_dimension=0, tiled=True
    ).astype(jnp.float32)
    back = summed.reshape(experts, capacity, width).astype(jnp.bfloat16)
    returned = lax.all_to_all(back, SP, split_axis=0, concat_axis=0, tiled=True)
    picked = returned.reshape(experts * capacity, width)[own_slots]
    picked = picked.astype(jnp.float32).reshape(rows, top, width)
    routed = jnp.sum(picked * routing_weight[:, :, None], axis=1)
    return (middle_wide + routed).astype(jnp.bfloat16)


def solution(mesh):
    finer = Mesh(mesh.devices.reshape(8, 4, 2, mesh.shape["tp"]), ("sp_0", "sp_1", "sp_2", "tp"))
    in_specs = (
        P(SP_TP, None),
        P(SP, "tp"),
        P(SP, "tp"),
        P(SP, "tp"),
        P(SP, "tp"),
        P("tp", SP),
        P("tp", SP),
        P("tp", SP),
        P(SP, "tp"),
        P(SP, "tp"),
        P(SP, "tp"),
        P(SP, "tp"),
        P("tp", SP),
        P("tp", SP),
        P("tp", SP),
        P("tp", None),
        P("tp", None),
        P(),
        P(SP, None),
        P(SP_TP, None),
        P(SP, None, "tp"),
        P(SP, None, "tp"),
        P(SP, "tp", None),
    )
    out_specs = P(SP_TP, None)
    return jax.shard_map(
        on_device, mesh=finer, in_specs=in_specs, out_specs=out_specs, check_vma=False
    )
```

profile of v0, /device:TPU:2, one launch (start us, length us, event | category | flops | bytes accessed | tf_op | source)
XLA Modules:
  0.0 524.9 jit_solution(10180655389004550311)
XLA Ops:
  21.2 2.1 all-gather.4
  30.7 13.7 %all-gather.5 = f32[4,196,256]{2,1,0:T(8,128)S(1)} all-gather(f32[1,196,256]{2,1,0:T(8,128)S(1)} %bitcast.532), channel_id=3, replica_groups=mesh['sp_0'=8,'sp_1'=4,'sp_2'=2,'tp'=4] {'sp_1'}, dimensions={0}, use_global_device_ids=true | all-gather | bytes 1003520 | tf_op jit(solution)/shard_map/all_gather | solution.py:34
  64.7 2.5 concatenate.14
  82.3 28.2 %all-gather.12.cloned.1.call-done = f32[8,196,256]{2,1,0:T(8,128)} async-done(((f32[1,196,256]{2,1,0:T(8,128)}), f32[8,196,256]{2,1,0:T(8,128)}) %all-gather.12.cloned.1.call-update) | async-done | bytes 1605648 | tf_op jit(solution)/shard_map/all_gather | solution.py:34
  145.9 2.9 fusion.113
  148.8 3.9 fusion.33
  154.8 2.8 fusion.14
  157.6 2.5 multiply_reduce_fusion.1
  163.5 2.1 add_convert_fusion
  165.6 4.4 all-to-all-start
  171.6 21.0 %all-to-all-done = bf16[4,128,2048]{2,1,0:T(8,128)(2,1)} async-done(((bf16[4,128,2048]{2,1,0:T(8,128)(2,1)}), bf16[4,128,2048]{2,1,0:T(8,128)(2,1)}, u32[]{:S(2)}, u32[]{:S(2)}) %all-to-all-start) | async-done | bytes 2097184 | tf_op jit(solution)/shard_map/all_to_all | solution.py:65
  192.6 2.1 convert_reduce_fusion
  195.3 3.3 gather_fusion
  198.6 58.8 %all_to_all.15 = bf16[64,8,2048]{2,1,0:T(8,128)(2,1)} all-to-all(bf16[64,8,2048]{2,1,0:T(8,128)(2,1)} %bitcast.525), channel_id=1, replica_groups=mesh['sp_0'=8,'sp_1'=4,'sp_2'=2,'tp'=4] {'sp_0','sp_1','sp_2'}, dimensions={0} | all-to-all | bytes 4194304 | tf_op jit(solution)/shard_map/all_to_all | solution.py:266
  257.4 80.1 %all-gather.10.cloned.1.call-done = bf16[256,8,2048]{2,1,0:T(8,128)(2,1)} async-done(((bf16[64,8,2048]{2,1,0:T(8,128)(2,1)}), bf16[256,8,2048]{2,1,0:T(8,128)(2,1)}) %all-gather.10.cloned.1.call-update) | async-done | bytes 8388624 | tf_op jit(solution)/shard_map/all_gather | solution.py:267
  337.5 7.8 %fusion = f32[2048,512]{1,0:T(8,128)S(1)} fusion(bf16[256,8,2048]{2,1,0:T(8,128)(2,1)} %all-gather.10.cloned.1.call-done, bf16[1,2048,512]{2,1,0:T(8,128)(2,1)} %param.44), kind=kOutput, calls=%fused_computation.2 | convolution fusion | flops 4294967296 | bytes 14680064 | tf_op jit(solution)/shard_map/dot_general | solution.py:270
  345.3 5.7 %multiply_convert_fusion = bf16[2048,512]{1,0:T(8,128)(2,1)S(1)} fusion(f32[2048,512]{1,0:T(8,128)S(1)} %fusion, bf16[256,8,2048]{2,1,0:T(8,128)(2,1)S(1)} %copy-done.43, bf16[1,2048,512]{2,1,0:T(8,128)(2,1)S(1)} %copy-done.44), kind=kOutput, calls=%fused_computation.7 | convolution fusion | flops 4305453056 | bytes 16777216 | tf_op jit(solution)/shard_map/dot_general | solution.py:269
  351.0 6.7 %convolution_convert_fusion = bf16[4,64,8,2048]{3,2,1,0:T(8,128)(2,1)} fusion(bf16[4,64,8,512]{3,2,1,0:T(8,128)(2,1)S(1)} %bitcast.586, bf16[1,512,2048]{2,1,0:T(8,128)(2,1)S(1)} %copy-done), kind=kOutput, calls=%fused_computation.6 | convolution fusion | flops 4299161600 | bytes 12582912 | tf_op jit(solution)/shard_map/dot_general | solution.py:274
  357.8 84.2 %reduce-scatter.2.cloned.1.call-done = bf16[1,64,8,2048]{3,2,1,0:T(8,128)(2,1)} async-done(((bf16[4,64,8,2048]{3,2,1,0:T(8,128)(2,1)}), bf16[1,64,8,2048]{3,2,1,0:T(8,128)(2,1)}) %reduce-scatter.2.cloned.1.call-update) | async-done | bytes 2097168 | tf_op jit(solution)/shard_map/reduce_scatter | solution.py:277
  442.0 10.9 %all-to-all-start.2 = ((bf16[64,8,2048]{2,1,0:T(8,128)(2,1)}), bf16[64,8,2048]{2,1,0:T(8,128)(2,1)}, u32[]{:S(2)}, u32[]{:S(2)}) async-start(bf16[64,8,2048]{2,1,0:T(8,128)(2,1)} %bitcast.527), calls=%async_computation.3 | async-start | bytes 4194304 | tf_op jit(solution)/shard_map/all_to_all | solution.py:281
  453.3 50.7 %all-to-all-done.2 = bf16[64,8,2048]{2,1,0:T(8,128)(2,1)} async-done(((bf16[64,8,2048]{2,1,0:T(8,128)(2,1)}), bf16[64,8,2048]{2,1,0:T(8,128)(2,1)}, u32[]{:S(2)}, u32[]{:S(2)}) %all-to-all-start.2) | async-done | bytes 2097184 | tf_op jit(solution)/shard_map/all_to_all | solution.py:281
  504.0 5.2 gather_fusion.1
  509.3 3.3 reshape.2161
  512.6 4.8 multiply_reduce_fusion
  (247 shorter events, 68.1 us)
Async XLA Ops:
  6.5 344.5 %copy-start = (bf16[1,512,2048]{2,1,0:T(8,128)(2,1)S(1)}, bf16[1,512,2048]{2,1,0:T(8,128)(2,1)}, u32[]{:S(2)}) copy-start(bf16[1,512,2048]{2,1,0:T(8,128)(2,1)} %param.45) | copy-start | bytes 6291460
  6.5 104.0 %all-gather.12.cloned.1.call-start = ((), (), s32[]{:S(2)}) async-start(), calls=%async_computation.6 | async-start | bytes 1843200 | tf_op jit(solution)/shard_map/all_gather | solution.py:34
  17.2 13.4 %copy-start.4 = (bf16[512,256]{0,1:T(8,128)(2,1)}, bf16[512,256]{0,1:T(8,128)(2,1)S(1)}, u32[]{:S(2)}) copy-start(bf16[512,256]{0,1:T(8,128)(2,1)S(1)} %copy.71) | copy-start | bytes 786436
  44.5 18.4 %copy-start.30 = (f32[2]{0:T(128)}, f32[2]{0:T(128)S(1)}, u32[]{:S(2)}) copy-start(f32[2]{0:T(128)S(1)} %get-tuple-element.27) | copy-start | bytes 28
  45.0 17.9 %copy-start.23 = (f32[2]{0:T(128)}, f32[2]{0:T(128)S(1)}, u32[]{:S(2)}) copy-start(f32[2]{0:T(128)S(1)} %get-tuple-element.29) | copy-start | bytes 28
  45.0 17.9 %copy-start.24 = (f32[2]{0:T(128)}, f32[2]{0:T(128)S(1)}, u32[]{:S(2)}) copy-start(f32[2]{0:T(128)S(1)} %get-tuple-element.98) | copy-start | bytes 28
  45.0 17.9 %copy-start.25 = (f32[2]{0:T(128)}, f32[2]{0:T(128)S(1)}, u32[]{:S(2)}) copy-start(f32[2]{0:T(128)S(1)} %get-tuple-element.31) | copy-start | bytes 28
  45.0 17.9 %copy-start.26 = (f32[2]{0:T(128)}, f32[2]{0:T(128)S(1)}, u32[]{:S(2)}) copy-start(f32[2]{0:T(128)S(1)} %get-tuple-element.99) | copy-start | bytes 28
  45.6 17.3 %copy-start.27 = (f32[2]{0:T(128)}, f32[2]{0:T(128)S(1)}, u32[]{:S(2)}) copy-start(f32[2]{0:T(128)S(1)} %get-tuple-element.33) | copy-start | bytes 28
  45.6 17.3 %copy-start.28 = (f32[2]{0:T(128)}, f32[2]{0:T(128)S(1)}, u32[]{:S(2)}) copy-start(f32[2]{0:T(128)S(1)} %get-tuple-element.100) | copy-start | bytes 28
  45.6 17.3 %copy-start.36 = (f32[2]{0:T(128)}, f32[2]{0:T(128)S(1)}, u32[]{:S(2)}) copy-start(f32[2]{0:T(128)S(1)} %get-tuple-element.34) | copy-start | bytes 28
  45.6 17.3 %copy-start.39 = (f32[2]{0:T(128)}, f32[2]{0:T(128)S(1)}, u32[]{:S(2)}) copy-start(f32[2]{0:T(128)S(1)} %subtract_exponential_fusion.22) | copy-start | bytes 28
  64.6 15.5 %copy-start.12 = (f32[1,512]{1,0:T(1,128)S(1)}, f32[1,512]{1,0:T(1,128)}, u32[]{:S(2)}) copy-start(f32[1,512]{1,0:T(1,128)} %param.28) | copy-start | bytes 6148
  64.7 16.4 %copy-start.13 = (f32[2,512]{1,0:T(2,128)S(1)}, f32[2,512]{1,0:T(2,128)}, u32[]{:S(2)}) copy-start(f32[2,512]{1,0:T(2,128)} %param.35) | copy-start | bytes 12292
  82.3 66.5 %copy-start.10 = (bf16[512,128]{0,1:T(8,128)(2,1)S(1)}, bf16[512,128]{0,1:T(8,128)(2,1)}, u32[]{:S(2)}) copy-start(bf16[512,128]{0,1:T(8,128)(2,1)} %copy-done.9) | copy-start | bytes 393220
  82.3 66.5 %copy-start.14 = (f32[2,512]{1,0:T(2,128)S(1)}, f32[2,512]{1,0:T(2,128)}, u32[]{:S(2)}) copy-start(f32[2,512]{1,0:T(2,128)} %param.35) | copy-start | bytes 12292
  131.0 13.6 %copy-start.41 = (f32[2]{0:T(128)S(1)}, f32[2]{0:T(128)}, u32[]{:S(2)}) copy-start(f32[2]{0:T(128)} %get-tuple-element.23) | copy-start | bytes 28
  131.0 14.2 %copy-start.15 = (f32[2,512]{1,0:T(2,128)S(1)}, f32[2,512]{1,0:T(2,128)}, u32[]{:S(2)}) copy-start(f32[2,512]{1,0:T(2,128)} %fusion.9) | copy-start | bytes 12292
  165.6 27.1 %all-to-all-start = ((bf16[4,128,2048]{2,1,0:T(8,128)(2,1)}), bf16[4,128,2048]{2,1,0:T(8,128)(2,1)}, u32[]{:S(2)}, u32[]{:S(2)}) async-start(bf16[4,128,2048]{2,1,0:T(8,128)(2,1)} %bitcast.526), calls=%async_computation | async-start | bytes 4194304 | tf_op jit(solution)/shard_map/all_to_all | solution.py:65
  170.0 24.7 %copy-start.8 = (bf16[128,2048]{1,0:T(8,128)(2,1)S(1)}, bf16[128,2048]{1,0:T(8,128)(2,1)}, u32[]{:S(2)}) copy-start(bf16[128,2048]{1,0:T(8,128)(2,1)} %param.23) | copy-start | bytes 1572868
  170.0 167.5 %all-gather.10.cloned.1.call-start = ((), (), s32[]{:S(2)}) async-start(), calls=%async_computation.5 | async-start | bytes 10485760 | tf_op jit(solution)/shard_map/all_gather | solution.py:267
  171.6 23.4 %copy-start.19 = (f32[2048]{0:T(1024)S(1)}, f32[2048]{0:T(1024)}, u32[]{:S(2)}) copy-start(f32[2048]{0:T(1024)} %param.40) | copy-start | bytes 24580
  257.4 184.7 %reduce-scatter.2.cloned.1.call-start = ((), (), s32[]{:S(2)}) async-start(), calls=%async_computation.4 | async-start | bytes 10485760 | tf_op jit(solution)/shard_map/reduce_scatter | solution.py:277
  442.0 62.0 %all-to-all-start.2 = ((bf16[64,8,2048]{2,1,0:T(8,128)(2,1)}), bf16[64,8,2048]{2,1,0:T(8,128)(2,1)}, u32[]{:S(2)}, u32[]{:S(2)}) async-start(bf16[64,8,2048]{2,1,0:T(8,128)(2,1)} %bitcast.527), calls=%async_computation.3 | async-start | bytes 4194304 | tf_op jit(solution)/shard_map/all_to_all | solution.py:281
  (26 other events, 129.2 us)
Sparse Core Ops, SparseCore 0:
  67.4 43.1 all-gather.11
  257.5 79.9 all-gather.9
  357.9 84.0 reduce-scatter.1
where the time goes:
time: 527 us; the launch traced here: 525 us
  waiting for transfers between devices  264 us (50%)
  blocking collectives  74.6 us (14%)
  local copies, waits for them, and re-layouts  57 us (11%)
  between operations  47 us (9%)
  matrix products  36.9 us (7%)
  other arithmetic  29.5 us (6%)
  starting transfers between devices  15.6 us (3%)
    reduce_scatter x1, waiting for transfers between devices, on_device(): lax.psum_scatter(partial_out.astype(jnp.bfloat16), 'tp', scatter_dimensio...  84.2 us
    all_gather x1, waiting for transfers between devices, on_device(): piece = lax.all_gather(arrived[None], 'tp', axis=0, tiled=True)  80.1 us
    all_to_all x1, blocking collectives, on_device(): lax.all_to_all(outgoing, SP, split_axis=0, concat_axis=0, tiled=True)  58.8 us
    all_to_all x1, waiting for transfers between devices, on_device(): returned = lax.all_to_all(back, SP, split_axis=0, concat_axis=0, tiled=True)  50.7 us
    all_gather x1, waiting for transfers between devices, collected_together(): both, at, found = (lax.all_gather(jnp.concatenate(lines), axis), 0, {})  28.2 us
    all_to_all x1, waiting for transfers between devices, sent_and_summed(): lax.all_to_all(parts, axis, split_axis=0, concat_axis=0, tiled=True)  21 us
    squeeze x14, local copies, waits for them, and re-layouts, prefix_by_axis(): subtotal = combine(subtotal, jax.tree.map(lambda part: part[k], pieces))  16.5 us
    all_gather x2, blocking collectives, collected_together(): both, at, found = (lax.all_gather(jnp.concatenate(lines), axis), 0, {})  15.8 us
  transfers between devices with their start and end apart: 5, of which 5 were waited for; matrix products, arithmetic and copies ran while one was open for 3% of the time, Pallas kernels for 0%

commit v1 on v0

v1 whole, which is shorter than its diff:
```python
import functools
import math

import jax
import jax.numpy as jnp
from jax import lax
from jax.experimental import pallas as pl
from jax.experimental.pallas import tpu as pltpu
from jax.sharding import Mesh
from jax.sharding import PartitionSpec as P

SP = ("sp_0", "sp_1", "sp_2")
SP_TP = ("sp_0", "sp_1", "sp_2", "tp")

EPSILON = 1e-06
FLOOR_LOG = -1e30
LIMIT = 7.0
SLOPE = 1.702
HIGHEST = lax.Precision.HIGHEST
F32 = jnp.float32
BF16 = jnp.bfloat16

DKA, DVA, DKB, DVB = 128, 256, 64, 128
HEADS = 3
SLICE = 6
WEIGHT_PAIRS = [(0, 3), (3, 0), (1, 2), (2, 1)]
ROW_PAIRS = [(0, 1), (1, 0), (2, 3), (3, 2)]


def lane_scan(x, combine, identity):
    length = x.shape[1]
    lane = lax.broadcasted_iota(jnp.int32, x.shape, 1)
    step = 1
    while step < length:
        shifted = pltpu.roll(x, step, 1)
        x = combine(x, jnp.where(lane >= step, shifted, identity))
        step *= 2
    return x


def local_kernel(bk, bv, big, bfl, bfb, sk, sv, sig, sfl, sfb, out, rows, cols, gates, flat):
    length = bk.shape[0]
    gates[...] = jnp.zeros_like(gates)
    for at, (broad, slim) in enumerate(((big, sig), (bfl, sfl), (bfb, sfb))):
        gates[8 * at : 8 * at + 1, :] = broad[...]
        gates[8 * at + 1 : 8 * at + 3, :] = slim[...]
    forget = gates[8:16, :]
    logf = -(jnp.maximum(-forget, 0.0) + jnp.log1p(jnp.exp(-jnp.abs(forget)))) + gates[16:24, :]
    prefix = lane_scan(logf, jnp.add, 0.0)
    level = gates[0:8, :] - prefix
    peak = lane_scan(level, jnp.maximum, -jnp.inf)
    totals = prefix[:, length - 1 : length]
    top = peak[:, length - 1 : length]
    rows[...] = level
    cols[:, 0:8] = jnp.transpose(level)
    cols[:, 8:16] = jnp.transpose(peak)
    weights = jnp.transpose(jnp.exp(level - top))
    kw = (weights[:, 0:1] * (bk[...].astype(F32) * (1.0 / math.sqrt(DKA)))).astype(BF16)
    contract = (((0,), (0,)), ((), ()))
    memory = lax.dot_general(kw, bv[...], contract, preferred_element_type=F32)
    flat[0:128, :] = memory[:, 0:128]
    flat[128:256, :] = memory[:, 128:256]
    first = lax.broadcasted_iota(jnp.int32, sk.shape, 1) < DKB
    both = jnp.where(first, weights[:, 1:2], weights[:, 2:3])
    kw = (both * (sk[...].astype(F32) * (1.0 / math.sqrt(DKB)))).astype(BF16)
    memory = lax.dot_general(kw, sv[...], contract, preferred_element_type=F32)
    flat[256:320, :] = memory[0:64, 0:128]
    flat[320:384, :] = memory[64:128, 128:256]
    ends = jnp.concatenate([totals, totals + top, jnp.zeros((8, 126), F32)], axis=1)
    line = jnp.zeros((1, 128), F32)
    lane = lax.broadcasted_iota(jnp.int32, (1, 128), 1)
    for h in range(HEADS):
        line = jnp.where(lane == h, ends[h : h + 1, 0:1], line)
        line = jnp.where(lane == 3 + h, ends[h : h + 1, 1:2], line)
    tail = jnp.concatenate([line, jnp.zeros((1, 128), F32)], axis=0)
    for p in range(out.shape[0]):
        out[p, 0:SLICE, :] = flat[SLICE * p : SLICE * p + SLICE, :]
        out[p, SLICE:8, :] = tail


def scan_kernel(place, arrived, out):
    count = arrived.shape[0]
    sub = lax.broadcasted_iota(jnp.int32, (8, 128), 0)
    row = sub + SLICE * place[0]
    is_first, is_second = (row < 256, row < 320)
    lane = lax.broadcasted_iota(jnp.int32, (8, 128), 1)

    def spread(line, at):
        return jnp.where(
            is_first,
            line[:, at : at + 1],
            jnp.where(is_second, line[:, at + 1 : at + 2], line[:, at + 2 : at + 3]),
        )

    memory = jnp.zeros((8, 128), F32)
    level = jnp.full((8, 128), FLOOR_LOG, F32)
    levels = [jnp.full((1, 1), FLOOR_LOG, F32) for _ in range(HEADS)]
    for s in range(count):
        tail = jnp.where(
            lane == 0, levels[0], jnp.where(lane == 1, levels[1], levels[2])
        )
        out[s] = jnp.where(sub < SLICE, memory, tail)
        if s == count - 1:
            break
        line = arrived[s, SLICE : SLICE + 1, :]
        total, local = (spread(line, 0), spread(line, 3))
        later = jnp.maximum(total + level, local)
        memory = jnp.exp(total + level - later) * memory + jnp.exp(local - later) * arrived[s]
        level = later
        levels = [
            jnp.maximum(line[:, h : h + 1] + levels[h], line[:, 3 + h : 4 + h])
            for h in range(HEADS)
        ]


def inside_kernel(bq, bk, bv, sq, sk, sv, rows, cols, routes, out, slots):
    length = bq.shape[0]
    first = lax.broadcasted_iota(jnp.int32, sq.shape, 1) < DKB
    zero = jnp.zeros_like(sq)
    groups = (
        (bq[...], bk, bv, 0, DVA, math.sqrt(DKA)),
        (jnp.where(first, sq[...], zero), sk, sv, 0, DVB, math.sqrt(DKB)),
        (jnp.where(first, zero, sq[...]), sk, sv, DVB, DVB, math.sqrt(DKB)),
    )
    step = 128
    at = 0
    for h, (query, key, value, offset, width, root) in enumerate(groups):
        for i in range(length // step):
            upto = step * (i + 1)
            mine = slice(step * i, upto)
            scores = lax.dot_general(
                query[mine, :], key[0:upto, :], (((1,), (1,)), ((), ())), preferred_element_type=F32
            )
            gap = rows[h : h + 1, 0:upto] - cols[mine, 8 + h : 9 + h]
            t = lax.broadcasted_iota(jnp.int32, (step, upto), 0) + step * i
            s = lax.broadcasted_iota(jnp.int32, (step, upto), 1)
            decay = jnp.exp(jnp.where(t >= s, gap, -jnp.inf))
            chosen = (decay * (scores * (1.0 / root))).astype(BF16)
            out[mine, at : at + width] = jnp.dot(
                chosen, value[0:upto, offset : offset + width], preferred_element_type=F32
            )
        at += width
    count = routes.shape[0]
    experts = lax.broadcasted_iota(jnp.int32, (count, 128), 1)
    one = (routes[:, 0:1] == experts).astype(F32)
    two = (routes[:, 1:2] == experts).astype(F32)
    lower = (
        lax.broadcasted_iota(jnp.int32, (count, count), 0)
        > lax.broadcasted_iota(jnp.int32, (count, count), 1)
    ).astype(BF16)
    before = jnp.dot(lower, one.astype(BF16), preferred_element_type=F32)
    rank = jnp.sum(before * one, axis=1, keepdims=True).astype(jnp.int32)
    slots[:, 0:1] = routes[:, 0:1] * 8 + rank
    before = jnp.dot(lower, two.astype(BF16), preferred_element_type=F32)
    before = before + jnp.sum(one, axis=0, keepdims=True)
    rank = jnp.sum(before * two, axis=1, keepdims=True).astype(jnp.int32)
    slots[:, 1:2] = routes[:, 1:2] * 8 + rank


def read_kernel(state, cols, inside, bq, sq, bgate, sgate, bweight, sweight, out, flat, mixed):
    for p in range(state.shape[0]):
        flat[SLICE * p : SLICE * p + SLICE, :] = state[p, 0:SLICE, :]
    line = state[0, SLICE : SLICE + 1, :]
    first = lax.broadcasted_iota(jnp.int32, sq.shape, 1) < DKB
    wide = sq[...].astype(F32)
    query = bq[...].astype(F32)
    broad = jnp.concatenate(
        [
            jnp.dot(query, flat[0:128, :], precision=HIGHEST, preferred_element_type=F32),
            jnp.dot(query, flat[128:256, :], precision=HIGHEST, preferred_element_type=F32),
        ],
        axis=1,
    )
    both = flat[256:384, :]
    carried = (
        broad,
        jnp.dot(
            jnp.where(first, wide, 0.0), both, precision=HIGHEST, preferred_element_type=F32
        ),
        jnp.dot(
            jnp.where(first, 0.0, wide), both, precision=HIGHEST, preferred_element_type=F32
        ),
    )
    gates = (bgate[...], sgate[:, 0:DVB], sgate[:, DVB : 2 * DVB])
    at = 0
    for h in range(HEADS):
        width = carried[h].shape[1]
        peak = cols[:, 8 + h : 9 + h]
        level = line[:, h : h + 1]
        top = jnp.maximum(level, peak)
        cell = jnp.exp(level - top) * carried[h] + jnp.exp(peak - top) * inside[:, at : at + width]
        square = jnp.mean(cell * cell, axis=1, keepdims=True)
        normed = cell * lax.rsqrt(square + EPSILON)
        mixed[:, at : at + width] = (normed * jax.nn.sigmoid(gates[h].astype(F32))).astype(BF16)
        at += width
    out[...] = (
        jnp.dot(mixed[:, 0:DVA], bweight[...], preferred_element_type=F32)
        + jnp.dot(mixed[:, DVA : 2 * DVA], sweight[...], preferred_element_type=F32)
    ).astype(BF16)


def middle_kernel(stream, parts, gain, slots, middle, outgoing):
    total = parts[0].astype(F32)
    for j in range(1, parts.shape[0]):
        total = total + parts[j].astype(F32)
    rounded = (stream[...].astype(F32) + total).astype(BF16)
    middle[...] = rounded
    wide = rounded.astype(F32)
    square = jnp.mean(wide * wide, axis=1, keepdims=True)
    normed = (wide * lax.rsqrt(square + EPSILON) * gain[...]).astype(BF16)
    count = normed.shape[0]
    lane = lax.broadcasted_iota(jnp.int32, (count, outgoing.shape[0]), 1)
    named = jnp.logical_or(slots[:, 0:1] == lane, slots[:, 1:2] == lane)
    outgoing[...] = lax.dot_general(
        named.astype(F32).astype(BF16),
        normed,
        (((0,), (0,)), ((), ())),
        preferred_element_type=F32,
    ).astype(BF16)


def combine_kernel(middle, returned, slots, weight, out):
    count = middle.shape[0]
    lane = lax.broadcasted_iota(jnp.int32, (count, returned.shape[0]), 1)
    total = jnp.zeros(middle.shape, F32)
    for k in range(2):
        picked = jnp.dot(
            (slots[:, k : k + 1] == lane).astype(F32).astype(BF16),
            returned[...],
            preferred_element_type=F32,
        )
        total = total + picked * weight[:, k : k + 1]
    out[...] = (middle[...].astype(F32) + total).astype(BF16)


def shape(dims, dtype):
    return jax.ShapeDtypeStruct(dims, dtype)


def activation(rows, gate_weight, linear_weight):
    gate_pre = jnp.dot(rows, gate_weight, preferred_element_type=F32)
    lin_pre = jnp.dot(rows, linear_weight, preferred_element_type=F32)
    glu = jnp.minimum(gate_pre, LIMIT)
    linear = jnp.clip(lin_pre, -LIMIT, LIMIT)
    return (glu * jax.nn.sigmoid(SLOPE * glu) * (linear + 1.0)).astype(BF16)


def on_device(
    stream,
    broad_queries,
    broad_keys,
    broad_values,
    broad_output_gate,
    broad_input_gate,
    broad_forget_logits,
    broad_forget_boost,
    slim_queries,
    slim_keys,
    slim_values,
    slim_output_gate,
    slim_input_gate,
    slim_forget_logits,
    slim_forget_boost,
    broad_output_weight,
    slim_output_weight,
    expert_norm_gain,
    routes,
    routing_weight,
    expert_gate_weight,
    expert_linear_weight,
    expert_down_weight,
):
    count = lax.axis_size(SP)
    tp_count = lax.axis_size("tp")
    place = lax.axis_index(SP)
    own = lax.axis_index("tp")
    length = broad_queries.shape[0]
    rows, width = stream.shape
    capacity = 8

    gate_own, linear_own = (expert_gate_weight[0], expert_linear_weight[0])
    gate_other = lax.ppermute(gate_own, "tp", WEIGHT_PAIRS)
    linear_other = lax.ppermute(linear_own, "tp", WEIGHT_PAIRS)
    down_all = lax.all_gather(expert_down_weight, "tp", axis=0, tiled=True)

    payload, level_rows, level_cols = pl.pallas_call(
        local_kernel,
        out_shape=(
            shape((count, 8, 128), F32),
            shape((8, length), F32),
            shape((length, 16), F32),
        ),
        scratch_shapes=[pltpu.VMEM((24, length), F32), pltpu.VMEM((SLICE * 64, 128), F32)],
        name="local",
    )(
        broad_keys,
        broad_values,
        broad_input_gate,
        broad_forget_logits,
        broad_forget_boost,
        slim_keys,
        slim_values,
        slim_input_gate,
        slim_forget_logits,
        slim_forget_boost,
    )
    arrived = lax.all_to_all(payload, SP, split_axis=0, concat_axis=0, tiled=True)
    own_routes = lax.dynamic_slice_in_dim(routes, own * rows, rows, 0)
    inside, slots = pl.pallas_call(
        inside_kernel,
        out_shape=(shape((length, 512), F32), shape((rows, 2), jnp.int32)),
        name="inside",
    )(
        broad_queries,
        broad_keys,
        broad_values,
        slim_queries,
        slim_keys,
        slim_values,
        level_rows,
        level_cols,
        own_routes,
    )
    entering = pl.pallas_call(
        scan_kernel,
        out_shape=shape((count, 8, 128), F32),
        in_specs=[
            pl.BlockSpec(memory_space=pltpu.SMEM),
            pl.BlockSpec(memory_space=pltpu.VMEM),
        ],
        name="scan",
    )(place.reshape(1), arrived)
    state = lax.all_to_all(entering, SP, split_axis=0, concat_axis=0, tiled=True)
    part = pl.pallas_call(
        read_kernel,
        out_shape=shape((length, width), BF16),
        scratch_shapes=[pltpu.VMEM((SLICE * 64, 128), F32), pltpu.VMEM((length, 512), BF16)],
        name="read",
    )(
        state,
        level_cols,
        inside,
        broad_queries,
        slim_queries,
        broad_output_gate,
        slim_output_gate,
        broad_output_weight,
        slim_output_weight,
    )
    parts = lax.all_to_all(
        part.reshape(tp_count, rows, width), "tp", split_axis=0, concat_axis=0, tiled=True
    )
    middle, outgoing = pl.pallas_call(
        middle_kernel,
        out_shape=(shape((rows, width), BF16), shape((count * capacity, width), BF16)),
        name="middle",
    )(stream, parts, expert_norm_gain.reshape(1, width), slots)
    dispatched = lax.all_to_all(
        outgoing.reshape(count, capacity, width), SP, split_axis=0, concat_axis=0, tiled=True
    ).reshape(count * capacity, width)
    partner_rows = lax.ppermute(dispatched, "tp", ROW_PAIRS)
    sent = jnp.stack(
        [
            activation(partner_rows, gate_own, linear_own),
            activation(partner_rows, gate_other, linear_other),
        ]
    )
    received = lax.ppermute(sent, "tp", ROW_PAIRS)
    mine = (
        activation(dispatched, gate_own, linear_own),
        activation(dispatched, gate_other, linear_other),
    )
    other = own ^ 1
    out = (
        jnp.dot(mine[0], expert_down_weight[0], preferred_element_type=F32)
        + jnp.dot(
            mine[1],
            lax.dynamic_index_in_dim(down_all, 3 - own, 0, keepdims=False),
            preferred_element_type=F32,
        )
        + jnp.dot(
            received[0],
            lax.dynamic_index_in_dim(down_all, other, 0, keepdims=False),
            preferred_element_type=F32,
        )
        + jnp.dot(
            received[1],
            lax.dynamic_index_in_dim(down_all, 3 - other, 0, keepdims=False),
            preferred_element_type=F32,
        )
    ).astype(BF16)
    returned = lax.all_to_all(
        out.reshape(count, capacity, width), SP, split_axis=0, concat_axis=0, tiled=True
    ).reshape(count * capacity, width)
    return pl.pallas_call(
        combine_kernel, out_shape=shape((rows, width), BF16), name="combine"
    )(middle, returned, slots, routing_weight)


def solution(mesh):
    finer = Mesh(mesh.devices.reshape(8, 4, 2, mesh.shape["tp"]), ("sp_0", "sp_1", "sp_2", "tp"))
    in_specs = (
        P(SP_TP, None),
        P(SP, "tp"),
        P(SP, "tp"),
        P(SP, "tp"),
        P(SP, "tp"),
        P("tp", SP),
        P("tp", SP),
        P("tp", SP),
        P(SP, "tp"),
        P(SP, "tp"),
        P(SP, "tp"),
        P(SP, "tp"),
        P("tp", SP),
        P("tp", SP),
        P("tp", SP),
        P("tp", None),
        P("tp", None),
        P(),
        P(SP, None),
        P(SP_TP, None),
        P(SP, None, "tp"),
        P(SP, None, "tp"),
        P(SP, "tp", None),
    )
    out_specs = P(SP_TP, None)
    return jax.shard_map(
        on_device, mesh=finer, in_specs=in_specs, out_specs=out_specs, check_vma=False
    )
```

time: 527 us -> 383 us (0.73)
  waiting for transfers between devices: 264 us -> 150 us
  local copies, waits for them, and re-layouts: 57 us -> 4.23 us
  blocking collectives: 74.6 us -> 111 us
  between operations: 47 us -> 13.5 us
  other arithmetic: 29.5 us -> 0.1 us
  Pallas kernels: 0 us -> 27.6 us
  starting transfers between devices: 15.6 us -> 31.5 us
  matrix products: 36.9 us -> 44 us
    all_gather x2 -> x1, waiting for transfers between devices: 108 us -> 0.02 us  [on_device(): down_all = lax.all_gather(expert_down_weight, 'tp', axis=0, tiled=True)]
    reduce_scatter x1 -> x0, waiting for transfers between devices: 84.2 us -> none  [on_device(): lax.psum_scatter(partial_out.astype(jnp.bfloat16), 'tp', scatter_dimensio...]
    ppermute x0 -> x4, waiting for transfers between devices: none -> 79.1 us  [the longest x1 34.9 us: on_device(): linear_other = lax.ppermute(linear_own, 'tp', WEIGHT_PAIRS)]
    all_to_all x1 -> x2, blocking collectives: 58.8 us -> 111 us  [the longest x1 57.9 us: on_device(): lax.all_to_all(outgoing.reshape(count, capacity, width), SP, split_axis=0...]
    pallas_call x0 -> x6, Pallas kernels: none -> 27.6 us  [the longest x1 7.7 us: on_device(): pl.pallas_call(read_kernel, out_shape=shape((length, width), BF16), scrat...]
    squeeze x14 -> x0, local copies, waits for them, and re-layouts: 16.5 us -> none  [prefix_by_axis(): subtotal = combine(subtotal, jax.tree.map(lambda part: part[k], pieces))]
    all_gather x2 -> x0, blocking collectives: 15.8 us -> none  [collected_together(): both, at, found = (lax.all_gather(jnp.concatenate(lines), axis), 0, {})]
    all_to_all x2 -> x3, starting transfers between devices: 15.3 us -> 27.3 us  [the longest x1 12 us: on_device(): lax.all_to_all(payload, SP, split_axis=0, concat_axis=0, tiled=True)]
  transfers between devices with their start and end apart: 5 -> 8, of which waited for: 5 -> 7; matrix products, arithmetic and copies ran while one was open for 3% -> 10% of each run, Pallas kernels for 0% -> 6%
where the time goes in v1:
time: 383 us; the launch traced here: 382 us
  waiting for transfers between devices  150 us (39%)
  blocking collectives  111 us (29%)
  matrix products  44 us (11%)
  starting transfers between devices  31.5 us (8%)
  Pallas kernels  27.6 us (7%)
  between operations  13.5 us (4%)
  local copies, waits for them, and re-layouts  4.23 us (1%)
    all_to_all x1, blocking collectives, on_device(): lax.all_to_all(outgoing.reshape(count, capacity, width), SP, split_axis=0...  57.9 us
    all_to_all x1, blocking collectives, on_device(): lax.all_to_all(part.reshape(tp_count, rows, width), 'tp', split_axis=0, c...  53.5 us
    all_to_all x1, waiting for transfers between devices, on_device(): lax.all_to_all(out.reshape(count, capacity, width), SP, split_axis=0, con...  50.5 us
    ppermute x1, waiting for transfers between devices, on_device(): linear_other = lax.ppermute(linear_own, 'tp', WEIGHT_PAIRS)  34.9 us
    ppermute x1, waiting for transfers between devices, on_device(): partner_rows = lax.ppermute(dispatched, 'tp', ROW_PAIRS)  31.9 us
    dot_general x4, matrix products, activation(): gate_pre = jnp.dot(rows, gate_weight, preferred_element_type=F32)  14 us
    all_to_all x1, waiting for transfers between devices, on_device(): lax.all_to_all(payload, SP, split_axis=0, concat_axis=0, tiled=True)  12.2 us
    all_to_all x1, starting transfers between devices, on_device(): lax.all_to_all(payload, SP, split_axis=0, concat_axis=0, tiled=True)  12 us
  transfers between devices with their start and end apart: 8, of which 7 were waited for; matrix products, arithmetic and copies ran while one was open for 10% of the time, Pallas kernels for 6%

profile of v1, /device:TPU:2, one launch (start us, length us, event | category | flops | bytes accessed | tf_op | source)
XLA Modules:
  0.0 382.3 jit_solution(8869757112528704248)
XLA Ops:
  7.3 3.9 %local.1 = (f32[64,8,128]{2,1,0:T(8,128)}, f32[8,512]{1,0:T(8,128)}, f32[512,16]{1,0:T(8,128)}) custom-call(bf16[512,128]{1,0:T(8,128)(2,1)} %bk.3, bf16[512,256]{1,0:T(8,128)(2,1)} %bv.3, f32[1,512]{1,0:T(1,128)} %big.1, f32[1,512]{1,0:T(1,128)} %bfl.1, f32[1,512]{1,0:T(1,128)} %bfb.1, bf16[512,128]{1,0:T(8,128)(2,1)} %sk.3, bf16[512,256]{1,0:T(8,128)(2,1)} %sv.3, ...), custom_call_target="tpu_custom_call" | custom-call | tf_op jit(solution)/shard_map/local/pallas_call | solution.py:286
  11.2 12.0 %all-to-all-start = ((f32[64,8,128]{2,1,0:T(8,128)}), f32[64,8,128]{2,1,0:T(8,128)S(1)}, u32[]{:S(2)}, u32[]{:S(2)}) async-start(f32[64,8,128]{2,1,0:T(8,128)} %get-tuple-element.12), calls=%async_computation | async-start | bytes 524288 | tf_op jit(solution)/shard_map/all_to_all | solution.py:307
  23.2 12.2 %all-to-all-done.arrived = f32[64,8,128]{2,1,0:T(8,128)S(1)} async-done(((f32[64,8,128]{2,1,0:T(8,128)}), f32[64,8,128]{2,1,0:T(8,128)S(1)}, u32[]{:S(2)}, u32[]{:S(2)}) %all-to-all-start) | async-done | bytes 262176 | tf_op jit(solution)/shard_map/all_to_all | solution.py:307
  36.1 4.4 %scan.1 = f32[64,8,128]{2,1,0:T(8,128)} custom-call(s32[1]{0:T(128)} %bitcast.place, f32[64,8,128]{2,1,0:T(8,128)} %copy-done.5), custom_call_target="tpu_custom_call" | custom-call | tf_op jit(solution)/shard_map/scan/pallas_call | solution.py:324
  40.5 5.7 %all-to-all-start.1 = ((f32[64,8,128]{2,1,0:T(8,128)}), f32[64,8,128]{2,1,0:T(8,128)S(1)}, u32[]{:S(2)}, u32[]{:S(2)}) async-start(f32[64,8,128]{2,1,0:T(8,128)} %scan.1), calls=%async_computation.1 | async-start | bytes 524288 | tf_op jit(solution)/shard_map/all_to_all | solution.py:333
  46.9 3.9 %inside.1 = (f32[512,512]{1,0:T(8,128)}, s32[128,2]{1,0:T(8,128)}) custom-call(bf16[512,128]{1,0:T(8,128)(2,1)} %bq.3, bf16[512,128]{1,0:T(8,128)(2,1)} %bk.3, bf16[512,256]{1,0:T(8,128)(2,1)} %bv.3, bf16[512,128]{1,0:T(8,128)(2,1)} %sq.3, bf16[512,128]{1,0:T(8,128)(2,1)} %sk.3, bf16[512,256]{1,0:T(8,128)(2,1)} %sv.3, f32[8,512]{1,0:T(8,128)} %get-tuple-element.14.rows, ...), custom_call_target="tpu_custom_call" | custom-call | tf_op jit(solution)/shard_map/inside/pallas_call | solution.py:309
  50.8 7.5 %all-to-all-done.1.state = f32[64,8,128]{2,1,0:T(8,128)S(1)} async-done(((f32[64,8,128]{2,1,0:T(8,128)}), f32[64,8,128]{2,1,0:T(8,128)S(1)}, u32[]{:S(2)}, u32[]{:S(2)}) %all-to-all-start.1) | async-done | bytes 262176 | tf_op jit(solution)/shard_map/all_to_all | solution.py:333
  59.0 7.7 %read.1 = bf16[512,2048]{1,0:T(8,128)(2,1)} custom-call(f32[64,8,128]{2,1,0:T(8,128)} %copy-done.4, f32[512,16]{1,0:T(8,128)} %get-tuple-element.13.cols, f32[512,512]{1,0:T(8,128)} %get-tuple-element.15.inside, bf16[512,128]{1,0:T(8,128)(2,1)} %bq.3, bf16[512,128]{1,0:T(8,128)(2,1)} %sq.3, bf16[512,256]{1,0:T(8,128)(2,1)} %bgate.1, bf16[512,256]{1,0:T(8,128)(2,1)} %sgate.1, ...), custom_call_target="tpu_custom_call" | custom-call | tf_op jit(solution)/shard_map/read/pallas_call | solution.py:334
  66.7 53.5 %all_to_all.25.parts = bf16[4,128,2048]{2,1,0:T(8,128)(2,1)} all-to-all(bf16[4,128,2048]{2,1,0:T(8,128)(2,1)} %bitcast.61), channel_id=1, replica_groups=mesh['sp_0'=8,'sp_1'=4,'sp_2'=2,'tp'=4] {'tp'}, dimensions={0} | all-to-all | bytes 4194304 | tf_op jit(solution)/shard_map/all_to_all | solution.py:350
  120.3 4.4 %middle.1 = (bf16[128,2048]{1,0:T(8,128)(2,1)}, bf16[512,2048]{1,0:T(8,128)(2,1)}) custom-call(bf16[128,2048]{1,0:T(8,128)(2,1)} %stream.1, bf16[4,128,2048]{2,1,0:T(8,128)(2,1)} %all_to_all.25.parts, f32[1,2048]{1,0:T(1,128)} %bitcast.64, s32[128,2]{1,0:T(8,128)} %get-tuple-element.16.slots), custom_call_target="tpu_custom_call" | custom-call | tf_op jit(solution)/shard_map/middle/pallas_call | solution.py:353
  124.7 57.9 %all_to_all.26 = bf16[64,8,2048]{2,1,0:T(8,128)(2,1)} all-to-all(bf16[64,8,2048]{2,1,0:T(8,128)(2,1)} %bitcast.63), channel_id=1, replica_groups=mesh['sp_0'=8,'sp_1'=4,'sp_2'=2,'tp'=4] {'sp_0','sp_1','sp_2'}, dimensions={0} | all-to-all | bytes 4194304 | tf_op jit(solution)/shard_map/all_to_all | solution.py:358
  186.5 3.6 convolution_minimum_fusion.3
  190.1 6.7 %fusion.9 = f32[512,2048]{1,0:T(8,128)} fusion(bf16[1,512,2048]{2,1,0:T(8,128)(2,1)S(1)} %copy-done.3, f32[512,512]{1,0:T(8,128)S(1)} %convolution_minimum_fusion.3, bf16[1,2048,512]{2,1,0:T(8,128)(2,1)} %param.44, bf16[64,8,2048]{2,1,0:T(8,128)(2,1)} %all_to_all.26), kind=kOutput, calls=%fused_computation.8 | convolution fusion | flops 2149842944 | bytes 11534336 | tf_op jit(solution)/shard_map/dot_general | solution.py:375
  196.8 31.9 %collective-permute-done.2 = bf16[512,2048]{1,0:T(8,128)(2,1)} collective-permute-done((bf16[512,2048]{1,0:T(8,128)(2,1)}, bf16[512,2048]{1,0:T(8,128)(2,1)}, u32[]{:S(2)}, u32[]{:S(2)}) %collective-permute-start.2) | collective-permute-done | bytes 2097184 | tf_op jit(solution)/shard_map/ppermute | solution.py:361
  228.7 3.5 convolution_minimum_fusion.1
  233.3 3.5 convolution_minimum_fusion
  236.8 3.6 fusion.22
  240.4 34.9 %collective-permute-done.1 = bf16[2048,512]{1,0:T(8,128)(2,1)} collective-permute-done((bf16[2048,512]{1,0:T(8,128)(2,1)}, bf16[2048,512]{1,0:T(8,128)(2,1)}, u32[]{:S(2)}, u32[]{:S(2)}) %collective-permute-start.1) | collective-permute-done | bytes 2097184 | tf_op jit(solution)/shard_map/ppermute | solution.py:283
  275.2 3.6 fusion.23
  282.7 7.3 %fusion.7 = f32[512,2048]{1,0:T(8,128)} fusion(bf16[4,512,2048]{2,1,0:T(8,128)(2,1)} %all-gather.2.cloned.1.call-done, s32[]{:T(128)S(6)} %select_n.14, f32[512,512]{1,0:T(8,128)S(1)} %convolution_minimum_fusion.2, bf16[2048,512]{1,0:T(8,128)(2,1)} %collective-permute-done.1, bf16[64,8,2048]{2,1,0:T(8,128)(2,1)} %all_to_all.26), kind=kOutput, calls=%fused_computation.6 | convolution fusion | flops 2149842944 | bytes 11534340 | tf_op jit(solution)/shard_map/dot_general | solution.py:376
  290.0 11.2 %collective-permute-done.3 = bf16[2,512,512]{2,1,0:T(8,128)(2,1)S(1)} collective-permute-done((bf16[2,512,512]{2,1,0:T(8,128)(2,1)S(1)}, bf16[2,512,512]{2,1,0:T(8,128)(2,1)S(1)}, u32[]{:S(2)}, u32[]{:S(2)}) %collective-permute-start.3) | collective-permute-done | bytes 1048608 | tf_op jit(solution)/shard_map/ppermute | solution.py:368
  304.1 5.9 %fusion = bf16[64,8,2048]{2,1,0:T(8,128)(2,1)} fusion(f32[512,2048]{1,0:T(8,128)S(1)} %fusion.5, f32[512,2048]{1,0:T(8,128)S(1)} %copy-done.2, f32[512,2048]{1,0:T(8,128)} %fusion.7, bf16[4,512,2048]{2,1,0:T(8,128)(2,1)} %all-gather.2.cloned.1.call-done, s32[]{:T(128)S(6)} %select_n.16, bf16[2,512,512]{2,1,0:T(8,128)(2,1)S(1)} %collective-permute-done.3), kind=kOutput, calls=%fused_computation.1 | convolution fusion | flops 1077936128 | bytes 17301508 | tf_op jit(solution)/shard_map/dot_general | solution.py:386
  310.0 9.6 %all-to-all-start.4 = ((bf16[64,8,2048]{2,1,0:T(8,128)(2,1)}), bf16[64,8,2048]{2,1,0:T(8,128)(2,1)S(1)}, u32[]{:S(2)}, u32[]{:S(2)}) async-start(bf16[64,8,2048]{2,1,0:T(8,128)(2,1)} %fusion), calls=%async_computation.4 | async-start | bytes 4194304 | tf_op jit(solution)/shard_map/all_to_all | solution.py:392
  320.3 50.5 %all-to-all-done.4 = bf16[64,8,2048]{2,1,0:T(8,128)(2,1)S(1)} async-done(((bf16[64,8,2048]{2,1,0:T(8,128)(2,1)}), bf16[64,8,2048]{2,1,0:T(8,128)(2,1)S(1)}, u32[]{:S(2)}, u32[]{:S(2)}) %all-to-all-start.4) | async-done | bytes 2097184 | tf_op jit(solution)/shard_map/all_to_all | solution.py:392
  (29 shorter events, 20.0 us)
Async XLA Ops:
  6.5 39.6 %copy-start = (s32[512,2]{0,1:T(2,128)S(1)}, s32[512,2]{0,1:T(2,128)}, u32[]{:S(2)}) copy-start(s32[512,2]{0,1:T(2,128)} %param.41) | copy-start | bytes 12292
  6.5 276.1 %all-gather.2.cloned.1.call-start = ((), (), s32[]{:S(2)}) async-start(), calls=%async_computation.5 | async-start | bytes 10485760 | tf_op jit(solution)/shard_map/all_gather | solution.py:284
  11.2 24.2 %all-to-all-start = ((f32[64,8,128]{2,1,0:T(8,128)}), f32[64,8,128]{2,1,0:T(8,128)S(1)}, u32[]{:S(2)}, u32[]{:S(2)}) async-start(f32[64,8,128]{2,1,0:T(8,128)} %get-tuple-element.12), calls=%async_computation | async-start | bytes 524288 | tf_op jit(solution)/shard_map/all_to_all | solution.py:307
  35.4 0.7 copy-start.5
  40.5 17.9 %all-to-all-start.1 = ((f32[64,8,128]{2,1,0:T(8,128)}), f32[64,8,128]{2,1,0:T(8,128)S(1)}, u32[]{:S(2)}, u32[]{:S(2)}) async-start(f32[64,8,128]{2,1,0:T(8,128)} %scan.1), calls=%async_computation.1 | async-start | bytes 524288 | tf_op jit(solution)/shard_map/all_to_all | solution.py:333
  58.3 0.7 copy-start.4
  182.5 46.2 %collective-permute-start.2 = (bf16[512,2048]{1,0:T(8,128)(2,1)}, bf16[512,2048]{1,0:T(8,128)(2,1)}, u32[]{:S(2)}, u32[]{:S(2)}) collective-permute-start(bf16[512,2048]{1,0:T(8,128)(2,1)} %bitcast.4), channel_id=1, source_target_pairs={{0,1},{1,0},{2,3},{3,2},{4,5},{5,4},{6,7},{7,6},{8,9},{9,8},{10,11... | collective-permute-start | bytes 6291464 | tf_op jit(solution)/shard_map/ppermute | solution.py:361
  183.3 50.0 %collective-permute-start = (bf16[2048,512]{1,0:T(8,128)(2,1)}, bf16[2048,512]{1,0:T(8,128)(2,1)}, u32[]{:S(2)}, u32[]{:S(2)}) collective-permute-start(bf16[2048,512]{1,0:T(8,128)(2,1)} %bitcast.5), channel_id=1, source_target_pairs={{0,3},{3,0},{1,2},{2,1},{4,7},{7,4},{5,6},{6,5},{8,11},{11,8},{9,1... | collective-permute-start | bytes 6291464 | tf_op jit(solution)/shard_map/ppermute | solution.py:282
  183.8 91.4 %collective-permute-start.1 = (bf16[2048,512]{1,0:T(8,128)(2,1)}, bf16[2048,512]{1,0:T(8,128)(2,1)}, u32[]{:S(2)}, u32[]{:S(2)}) collective-permute-start(bf16[2048,512]{1,0:T(8,128)(2,1)} %bitcast.6), channel_id=1, source_target_pairs={{0,3},{3,0},{1,2},{2,1},{4,7},{7,4},{5,6},{6,5},{8,11},{11,8},{9,1... | collective-permute-start | bytes 6291464 | tf_op jit(solution)/shard_map/ppermute | solution.py:283
  186.5 3.6 copy-start.3
  279.0 22.3 %collective-permute-start.3 = (bf16[2,512,512]{2,1,0:T(8,128)(2,1)S(1)}, bf16[2,512,512]{2,1,0:T(8,128)(2,1)S(1)}, u32[]{:S(2)}, u32[]{:S(2)}) collective-permute-start(bf16[2,512,512]{2,1,0:T(8,128)(2,1)S(1)} %pad_maximum_fusion), channel_id=1, source_target_pairs={{0,1},{1,0},{2,3},{3,2},{4,5},{5,4},{6,7},{7,6},{8,9},{9,8},{10,11... | collective-permute-start | bytes 3145736 | tf_op jit(solution)/shard_map/ppermute | solution.py:368
  290.0 14.1 %copy-start.2 = (f32[512,2048]{1,0:T(8,128)S(1)}, f32[512,2048]{1,0:T(8,128)}, u32[]{:S(2)}) copy-start(f32[512,2048]{1,0:T(8,128)} %fusion.9) | copy-start | bytes 12582916
  310.0 9.6 %copy-start.6 = (f32[128,2]{0,1:T(2,128)S(1)}, f32[128,2]{0,1:T(2,128)}, u32[]{:S(2)}) copy-start(f32[128,2]{0,1:T(2,128)} %param.42) | copy-start | bytes 3076
  310.0 60.8 %all-to-all-start.4 = ((bf16[64,8,2048]{2,1,0:T(8,128)(2,1)}), bf16[64,8,2048]{2,1,0:T(8,128)(2,1)S(1)}, u32[]{:S(2)}, u32[]{:S(2)}) async-start(bf16[64,8,2048]{2,1,0:T(8,128)(2,1)} %fusion), calls=%async_computation.4 | async-start | bytes 4194304 | tf_op jit(solution)/shard_map/all_to_all | solution.py:392
  370.8 1.3 copy-start.1
Sparse Core Ops, SparseCore 0:
  9.1 111.0 all-gather.1
